TPU v7x, 1024 devices: a whole 4x8x16 slice. The times are simulated.
1024 devices in a mesh: fs: 16 (over z), rep: 8 (over y), tp: 8 (over x, core).
Axes of the slice: x: 4, y: 8, z: 16, core: 2. Of those that a mesh axis runs over, the one named last changes fastest.
Arguments:
- saved_hidden: bfloat16 [114688, 2048], P(('fs', 'rep')), may hold values from -12 to 12
- grad_value: bfloat16 [114688, 1024], P(('fs', 'rep'), 'tp'), may hold values from -12 to 12
- saved_mixed: bfloat16 [114688, 1024], P(('fs', 'rep'), 'tp'), may hold values from -12 to 12
- grad_output: bfloat16 [114688, 2048], P(('fs', 'rep')), may hold values from -12 to 12
- basis_value: bfloat16 [2048, 128], replicated, may hold values from -0.5 to 0.5
- basis_output: bfloat16 [2048, 128], replicated, may hold values from -0.5 to 0.5
- weight_value: float32 [2048, 1024], P('fs', 'tp'), may hold values from -0.125 to 0.125
- weight_output: float32 [1024, 2048], P('tp', 'fs'), may hold values from -0.1875 to 0.1875
- first_value: float32 [128, 1024], P('fs', 'tp'), may hold values from -4 to 4
- second_value: float32 [128, 1024], P('fs', 'tp'), may hold values from 0.05 to 0.5
- first_output: float32 [128, 1024], P('fs', 'tp'), may hold values from -4 to 4
- second_output: float32 [128, 1024], P('fs', 'tp'), may hold values from 0.05 to 0.5
Outputs:
- step_value: float32 [2048, 1024], P('fs', 'tp')
- step_output: float32 [1024, 2048], P('tp', 'fs')
- new_weight_value: float32 [2048, 1024], P('fs', 'tp')
- new_weight_output: float32 [1024, 2048], P('tp', 'fs')
- copy_value: bfloat16 [2048, 1024], P(None, 'tp')
- copy_output: bfloat16 [1024, 2048], P('tp')
- new_first_value: float32 [128, 1024], P('fs', 'tp')
- new_second_value: float32 [128, 1024], P('fs', 'tp')
- new_first_output: float32 [128, 1024], P('fs', 'tp')
- new_second_output: float32 [128, 1024], P('fs', 'tp')
All inputs are finite; a program needn't handle non-finite values.
Results may differ from a plain program's by a relative error of at most 0.0045.
Values may be sent and summed in bfloat16 or wider, within the bound.
No kernel may reach another device: no remote copies, remote signals or barrier semaphores. Data moves between devices by JAX's collectives and lax.ppermute only.
A program may use at most 32 MiB of HBM per device.

v0:
```python
import jax
import jax.numpy as jnp
from jax import lax
from jax.experimental import pallas as pl
from jax.experimental.pallas import tpu as pltpu
from jax.sharding import PartitionSpec as P


AW = 1024
RANK = 128


first_decay = 0.8
second_decay = 0.9
learning_rate = 0.02
norm_epsilon = 1e-06
f32 = jnp.float32
bf16 = jnp.bfloat16
contract_leading = (((0,), (0,)), ((), ()))
contract_trailing = (((1,), (1,)), ((), ()))


def exchange(chunks, axes):
    return lax.all_to_all(chunks, axes, 0, 0, tiled=True)


def split(array):
    upper = array.astype(bf16)
    return upper, (array - upper.astype(f32)).astype(bf16)


def moments(projected, first_old, second_old, clip_factor):
    scaled = clip_factor * projected
    first_new = first_decay * first_old + (1.0 - first_decay) * scaled
    second_new = second_decay * second_old + (1.0 - second_decay) * scaled * scaled
    return (first_new, second_new, first_new / jnp.sqrt(second_new))


def finish_kernel(
    fs_ref,
    rep_ref,
    rows_ref,
    squares_ref,
    whole_ref,
    first_value_ref,
    second_value_ref,
    first_output_ref,
    second_output_ref,
    basis_value_ref,
    basis_output_ref,
    weight_value_ref,
    weight_output_ref,
    *refs,
):
    rep = len(refs) - 14
    piece_refs, refs = refs[:rep], refs[rep:]
    (
        step_value_ref,
        step_output_ref,
        new_weight_value_ref,
        new_weight_output_ref,
        copy_value_ref,
        copy_output_ref,
        new_first_value_ref,
        new_second_value_ref,
        new_first_output_ref,
        new_second_output_ref,
        wholes_ref,
        olds_ref,
        value_ref,
        output_ref,
    ) = refs
    fs, _, columns = rows_ref.shape
    ranks = first_value_ref.shape[0]
    count = 2 * ranks
    block = weight_value_ref.shape[0]
    cut = block // rep
    part = 4 * ranks // rep
    run = min(part, ranks)
    for away in range(rep):
        other = lax.rem(rep_ref[0] + away, rep)
        wholes_ref[other] = piece_refs[away][:, : 2 * cut, :]
        old = piece_refs[away][:, 2 * cut :, :].astype(f32)
        olds_ref[other] = old[:, :part] + old[:, part:]

    total = squares_ref[0]
    for t in range(1, squares_ref.shape[0]):
        total = total + squares_ref[t]
    mean_square = jnp.max(total, keepdims=True) / (2 * RANK * AW)
    clip_factor = jnp.minimum(1.0, 1.0 / jnp.sqrt(mean_square + norm_epsilon))

    def old(i, k):
        runs = [
            olds_ref[at // part, i, at % part : at % part + run, :]
            for at in range(k * ranks, (k + 1) * ranks, run)
        ]
        return jnp.concatenate(runs) if len(runs) > 1 else runs[0]

    for i in range(fs):
        here = slice(i * ranks, (i + 1) * ranks)
        row = rows_ref[i, :count, :].astype(f32)
        value_ref[here, :] = moments(row[:ranks], old(i, 0), old(i, 1), clip_factor)[2]
        output_ref[here, :] = moments(row[ranks:], old(i, 2), old(i, 3), clip_factor)[2]
    first, second, _ = moments(
        whole_ref[:ranks, :], first_value_ref[...], second_value_ref[...], clip_factor
    )
    new_first_value_ref[...] = first
    new_second_value_ref[...] = second
    first, second, _ = moments(
        whole_ref[ranks:, :], first_output_ref[...], second_output_ref[...], clip_factor
    )
    new_first_output_ref[...] = first
    new_second_output_ref[...] = second

    value_upper, value_lower = split(value_ref[...])
    output_upper, output_lower = split(output_ref[...].T)

    def value_step(basis):
        return jnp.dot(basis, value_upper, preferred_element_type=f32) + jnp.dot(
            basis, value_lower, preferred_element_type=f32
        )

    def output_step(basis):
        return lax.dot_general(
            output_upper, basis, contract_trailing, preferred_element_type=f32
        ) + lax.dot_general(output_lower, basis, contract_trailing, preferred_element_type=f32)

    own = fs_ref[0]
    own_rows = pl.ds(pl.multiple_of(own * block, block), block)
    step = value_step(basis_value_ref[own_rows, :])
    step_value_ref[...] = step
    new_weight_value_ref[...] = weight_value_ref[...] - learning_rate * step
    step = output_step(basis_output_ref[own_rows, :])
    step_output_ref[...] = step
    new_weight_output_ref[...] = weight_output_ref[...] - learning_rate * step
    for i in range(fs):
        here = slice(i * block, (i + 1) * block)
        whole = wholes_ref[:, i, :cut, :].reshape(block, columns).astype(f32)
        step = value_step(basis_value_ref[here, :])
        copy_value_ref[here, :] = (whole - learning_rate * step).astype(bf16)
        whole = wholes_ref[:, i, cut:, :].reshape(block, columns).astype(f32)
        step = output_step(basis_output_ref[here, :])
        copy_output_ref[:, here] = (whole - learning_rate * step).astype(bf16)


vmem = pl.BlockSpec(memory_space=pltpu.VMEM)
smem = pl.BlockSpec(memory_space=pltpu.SMEM)


def call(kernel, inputs, shapes, specs=None, scratch=(), flops=0, room=8, grid=None):
    outs = tuple(jax.ShapeDtypeStruct(s, t) for s, t in shapes)
    more = {} if grid is None else {"grid": grid}
    return pl.pallas_call(
        kernel,
        out_shape=outs,
        in_specs=[vmem] * len(inputs) if specs is None else specs,
        out_specs=tuple(vmem for _ in outs),
        scratch_shapes=scratch,
        compiler_params=pltpu.CompilerParams(vmem_limit_bytes=room * 2**20),
        cost_estimate=pl.CostEstimate(flops=flops, bytes_accessed=2**20, transcendentals=0),
        **more,
    )(*inputs)


def split_product(reduced, other):
    stacked = jnp.concatenate(split(reduced), axis=1)
    return lax.dot_general(stacked, other, contract_leading, preferred_element_type=f32)


def partial_kernel(
    rep_ref,
    value_ref,
    output_ref,
    weight_value_ref,
    weight_output_ref,
    first_value_ref,
    second_value_ref,
    first_output_ref,
    second_output_ref,
    out_ref,
    old_ref,
):
    fs = out_ref.shape[0]
    ranks = first_value_ref.shape[0]
    count = 2 * ranks
    rep, part, _ = old_ref.shape
    cut = weight_value_ref.shape[0] // rep
    run = min(part, ranks)
    olds = (first_value_ref, second_value_ref, first_output_ref, second_output_ref)
    for at in range(0, 4 * ranks, run):
        from_row, to_row = at % ranks, at % part
        old_ref[at // part, to_row : to_row + run, :] = olds[at // ranks][
            from_row : from_row + run, :
        ]
    me = rep_ref[0]
    piece = pl.ds(pl.multiple_of(me * cut, cut), cut)
    piece_value = weight_value_ref[piece, :].astype(bf16)
    piece_output = weight_output_ref[piece, :].astype(bf16)
    old = old_ref[me]
    upper = old.astype(bf16).astype(f32)
    piece_old = jnp.concatenate([upper, old - upper]).astype(bf16)
    olds_at = count + 2 * cut
    for i in range(fs):
        here = slice(i * ranks, (i + 1) * ranks)
        there = slice(RANK + i * ranks, RANK + (i + 1) * ranks)
        value = value_ref[here, :] + value_ref[there, :]
        output = output_ref[here, :] + output_ref[there, :]
        out_ref[i, :count, :] = jnp.concatenate([value, output]).astype(bf16)
        out_ref[i, count : count + cut, :] = piece_value
        out_ref[i, count + cut : olds_at, :] = piece_output
        out_ref[i, olds_at:, :] = piece_old


def partial(rep_index, hidden, grad_value, grad_output, mixed, bases, weights, olds, fs, rep):
    rows, columns = weights[0].shape
    ranks = olds[0].shape[0]
    part = 4 * ranks // rep
    reduced_hidden = jnp.dot(hidden, bases[0], preferred_element_type=f32)
    reduced_output = jnp.dot(grad_output, bases[1], preferred_element_type=f32)
    value = split_product(reduced_hidden, grad_value)
    output = split_product(reduced_output, mixed)
    height = 2 * ranks + 2 * (rows // rep) + 2 * part
    return call(
        partial_kernel,
        (rep_index, value, output, *weights, *olds),
        [((fs, height, columns), bf16)],
        specs=[smem] + [vmem] * 8,
        scratch=[pltpu.VMEM((rep, part, columns), f32)],
    )[0]


def sum_kernel(mixed_ref, out_ref, pieces_ref):
    count = out_ref.shape[1]
    total = mixed_ref[0, :count, :].astype(f32)
    for i in range(1, mixed_ref.shape[0]):
        total = total + mixed_ref[i, :count, :].astype(f32)
    for j in range(out_ref.shape[0]):
        out_ref[j] = total
    pieces_ref[...] = mixed_ref[:, count:, :]


def rows_kernel(sums_ref, whole_ref, out_ref):
    total = sums_ref[0]
    for j in range(1, sums_ref.shape[0]):
        total = total + sums_ref[j]
    whole_ref[...] = total
    total = total.astype(bf16)
    for i in range(out_ref.shape[0]):
        out_ref[i] = total


def squares_kernel(rows_ref, out_ref):
    total = jnp.zeros(rows_ref.shape[1:], f32)
    for i in range(rows_ref.shape[0]):
        row = rows_ref[i].astype(f32)
        total = total + row * row
    total = jnp.sum(total, keepdims=True)
    out_ref[...] = jnp.broadcast_to(total[None], out_ref.shape)


def local(
    saved_hidden,
    grad_value,
    saved_mixed,
    grad_output,
    basis_value,
    basis_output,
    weight_value,
    weight_output,
    first_value,
    second_value,
    first_output,
    second_output,
):
    fs, rep, tp = lax.axis_size("fs"), lax.axis_size("rep"), lax.axis_size("tp")
    fs_index = lax.axis_index("fs").astype(jnp.int32).reshape(1)
    rep_index = lax.axis_index("rep").astype(jnp.int32).reshape(1)
    rows, columns = weight_value.shape
    ranks = first_value.shape[0]

    olds = (first_value, second_value, first_output, second_output)
    weights = (weight_value, weight_output)
    bases = (basis_value, basis_output)
    start = partial(
        rep_index,
        saved_hidden,
        grad_value,
        grad_output,
        saved_mixed,
        bases,
        weights,
        olds,
        fs,
        rep,
    )
    mixed = exchange(start, "fs")

    count = 2 * ranks
    height = mixed.shape[1] - count
    summed, piece = call(
        sum_kernel,
        (mixed,),
        [((rep, count, columns), f32), ((fs, height, columns), bf16)],
    )
    summed = exchange(summed, "rep")
    whole, rowed = call(
        rows_kernel, (summed,), [((count, columns), f32), ((fs, count, columns), bf16)]
    )

    gathered = exchange(rowed, "fs")
    squares = call(squares_kernel, (gathered,), [((tp, 8, columns), f32)])[0]
    squares = exchange(squares, "tp")

    pieces = [piece] + [None] * (rep - 1)
    up = down = piece
    for far in range(1, rep // 2 + 1):
        up = lax.ppermute(up, "rep", [(r, (r + 1) % rep) for r in range(rep)])
        pieces[rep - far] = up
        if 2 * far < rep:
            down = lax.ppermute(down, "rep", [(r, (r - 1) % rep) for r in range(rep)])
            pieces[far] = down

    depth = basis_value.shape[0]
    shapes = [((rows, columns), f32)] * 4
    shapes += [((depth, columns), bf16), ((rows, depth), bf16)] + [((ranks, columns), f32)] * 4
    return call(
        finish_kernel,
        (fs_index, rep_index, gathered, squares, whole, *olds, *bases, *weights, *pieces),
        shapes,
        specs=[smem] * 2 + [vmem] * (11 + rep),
        scratch=[
            pltpu.VMEM((rep, fs, 2 * (rows // rep), columns), bf16),
            pltpu.VMEM((rep, fs, 4 * ranks // rep, columns), f32),
        ]
        + [pltpu.VMEM((RANK, columns), f32)] * 2,
        flops=8 * depth * RANK * columns,
        room=16,
    )


def solution(mesh):
    return jax.shard_map(
        local,
        mesh=mesh,
        in_specs=(
            P(("fs", "rep"), None),
            P(("fs", "rep"), "tp"),
            P(("fs", "rep"), "tp"),
            P(("fs", "rep"), None),
            P(),
            P(),
            P("fs", "tp"),
            P("tp", "fs"),
            P("fs", "tp"),
            P("fs", "tp"),
            P("fs", "tp"),
            P("fs", "tp"),
        ),
        out_specs=(
            P("fs", "tp"),
            P("tp", "fs"),
            P("fs", "tp"),
            P("tp", "fs"),
            P(None, "tp"),
            P("tp", None),
            P("fs", "tp"),
            P("fs", "tp"),
            P("fs", "tp"),
            P("fs", "tp"),
        ),
        check_vma=False,
    )
```

profile of v0, /device:TPU:1, one launch (start us, length us, event | category | flops | bytes accessed | tf_op | source)
XLA Modules:
  0.0 102.4 jit_solution(1838492189645913660)
XLA Ops:
  0.6 0.0 copy-start
  0.7 0.0 copy-start.2
  0.7 0.0 copy-start.9
  0.7 3.5 %subtract_convert_fusion.1 = (bf16[896,128]{0,1:T(8,128)(2,1)S(1)}, bf16[896,128]{0,1:T(8,128)(2,1)S(1)}) fusion(bf16[896,2048]{1,0:T(8,128)(2,1)} %param.12, bf16[2048,128]{1,0:T(8,128)(2,1)} %basis_value_ref.1), kind=kOutput, calls=%fused_computation.9 | convolution fusion | flops 470220800 | bytes 4653056 | tf_op jit(solution)/shard_map/dot_general | solution.py:218
  4.2 0.0 copy-done.2
  4.2 0.0 copy-done.9
  4.2 0.0 copy-start.10
  4.2 0.0 copy-start.3
  4.2 0.0 copy-start.4
  4.3 0.0 copy-start.5
  4.3 0.0 copy-start.6
  4.3 0.0 copy-start.7
  4.3 0.0 copy-start.8
  4.3 0.0 copy-start.1
  4.3 1.2 %subtract_convert_fusion = (bf16[896,128]{0,1:T(8,128)(2,1)S(1)}, bf16[896,128]{0,1:T(8,128)(2,1)S(1)}) fusion(bf16[896,2048]{1,0:T(8,128)(2,1)S(1)} %copy-done.9, bf16[2048,128]{1,0:T(8,128)(2,1)S(1)} %copy-done.2), kind=kOutput, calls=%fused_computation.8 | convolution fusion | flops 470220800 | bytes 4653056 | tf_op jit(solution)/shard_map/dot_general | solution.py:219
  5.6 0.0 copy-done
  5.6 0.3 fusion.value_ref
  5.9 0.0 copy-done.10
  5.9 0.3 fusion.4.output_ref
  6.1 0.0 copy-done.3
  6.1 0.0 copy-done.4
  6.2 0.0 copy-done.5
  6.2 31.9 %all_to_all.20.mixed_ref = bf16[16,56,128]{2,1,0:T(8,128)(2,1)S(1)} all-to-all(bf16[16,56,128]{2,1,0:T(8,128)(2,1)S(1)} %shard_map.195), channel_id=1, replica_groups=mesh['fs'=16,'rep'=8,'tp'=8] {'fs'}, dimensions={0} | all-to-all | bytes 458752 | tf_op jit(solution)/shard_map/all_to_all | solution.py:24
  38.1 0.7 shard_map.196
  38.7 3.2 %collective-permute-start.3 = (bf16[16,40,128]{2,1,0:T(8,128)(2,1)S(1)}, bf16[16,40,128]{2,1,0:T(8,128)(2,1)S(1)}, u32[]{:S(2)}, u32[]{:S(2)}) collective-permute-start(bf16[16,40,128]{2,1,0:T(8,128)(2,1)S(1)} %get-tuple-element.17.refs_0_), channel_id=1, source_target_pairs={{0,8},{8,16},{16,24},{24,32},{32,40},{40,48},{48,56},{56,0},{1,9},... | collective-permute-start | bytes 491528 | tf_op jit(solution)/shard_map/ppermute | solution.py:317
  41.9 3.8 %collective-permute-start = (bf16[16,40,128]{2,1,0:T(8,128)(2,1)S(1)}, bf16[16,40,128]{2,1,0:T(8,128)(2,1)S(1)}, u32[]{:S(2)}, u32[]{:S(2)}) collective-permute-start(bf16[16,40,128]{2,1,0:T(8,128)(2,1)S(1)} %get-tuple-element.17.refs_0_), channel_id=1, source_target_pairs={{0,56},{8,0},{16,8},{24,16},{32,24},{40,32},{48,40},{56,48},{1,57}... | collective-permute-start | bytes 491528 | tf_op jit(solution)/shard_map/ppermute | solution.py:320
  45.8 0.8 collective-permute-done.3.refs_7_
  46.5 1.9 %collective-permute-start.4 = (bf16[16,40,128]{2,1,0:T(8,128)(2,1)S(1)}, bf16[16,40,128]{2,1,0:T(8,128)(2,1)S(1)}, u32[]{:S(2)}, u32[]{:S(2)}) collective-permute-start(bf16[16,40,128]{2,1,0:T(8,128)(2,1)S(1)} %collective-permute-done.3.refs_7_), channel_id=1, source_target_pairs={{0,8},{8,16},{16,24},{24,32},{32,40},{40,48},{48,56},{56,0},{1,9},... | collective-permute-start | bytes 491528 | tf_op jit(solution)/shard_map/ppermute | solution.py:317
  48.4 6.6 %all-to-all-start.1 = ((f32[8,16,128]{2,1,0:T(8,128)}), f32[8,16,128]{2,1,0:T(8,128)S(1)}, u32[]{:S(2)}, u32[]{:S(2)}) async-start(f32[8,16,128]{2,1,0:T(8,128)} %get-tuple-element.14), calls=%async_computation.1 | async-start | bytes 131072 | tf_op jit(solution)/shard_map/all_to_all | solution.py:24
  55.0 0.0 collective-permute-done.refs_1_
  55.0 4.6 %collective-permute-start.1 = (bf16[16,40,128]{2,1,0:T(8,128)(2,1)S(1)}, bf16[16,40,128]{2,1,0:T(8,128)(2,1)S(1)}, u32[]{:S(2)}, u32[]{:S(2)}) collective-permute-start(bf16[16,40,128]{2,1,0:T(8,128)(2,1)S(1)} %collective-permute-done.refs_1_), channel_id=1, source_target_pairs={{0,56},{8,0},{16,8},{24,16},{32,24},{40,32},{48,40},{56,48},{1,57}... | collective-permute-start | bytes 491528 | tf_op jit(solution)/shard_map/ppermute | solution.py:320
  59.6 0.0 collective-permute-done.4.refs_6_
  59.6 1.9 %collective-permute-start.5 = (bf16[16,40,128]{2,1,0:T(8,128)(2,1)S(1)}, bf16[16,40,128]{2,1,0:T(8,128)(2,1)S(1)}, u32[]{:S(2)}, u32[]{:S(2)}) collective-permute-start(bf16[16,40,128]{2,1,0:T(8,128)(2,1)S(1)} %collective-permute-done.4.refs_6_), channel_id=1, source_target_pairs={{0,8},{8,16},{16,24},{24,32},{32,40},{40,48},{48,56},{56,0},{1,9},... | collective-permute-start | bytes 491528 | tf_op jit(solution)/shard_map/ppermute | solution.py:317
  61.6 1.0 %all-to-all-done.1.sums_ref = f32[8,16,128]{2,1,0:T(8,128)S(1)} async-done(((f32[8,16,128]{2,1,0:T(8,128)}), f32[8,16,128]{2,1,0:T(8,128)S(1)}, u32[]{:S(2)}, u32[]{:S(2)}) %all-to-all-start.1) | async-done | bytes 65568 | tf_op jit(solution)/shard_map/all_to_all | solution.py:24
  62.6 0.6 shard_map.197
  63.2 10.6 %all-to-all-start.2 = ((bf16[16,16,128]{2,1,0:T(8,128)(2,1)}), bf16[16,16,128]{2,1,0:T(8,128)(2,1)S(1)}, u32[]{:S(2)}, u32[]{:S(2)}) async-start(bf16[16,16,128]{2,1,0:T(8,128)(2,1)} %get-tuple-element.15), calls=%async_computation.2 | async-start | bytes 131072 | tf_op jit(solution)/shard_map/all_to_all | solution.py:24
  73.9 0.0 collective-permute-done.1.refs_2_
  73.9 3.9 %collective-permute-start.2 = (bf16[16,40,128]{2,1,0:T(8,128)(2,1)S(1)}, bf16[16,40,128]{2,1,0:T(8,128)(2,1)S(1)}, u32[]{:S(2)}, u32[]{:S(2)}) collective-permute-start(bf16[16,40,128]{2,1,0:T(8,128)(2,1)S(1)} %collective-permute-done.1.refs_2_), channel_id=1, source_target_pairs={{0,56},{8,0},{16,8},{24,16},{32,24},{40,32},{48,40},{56,48},{1,57}... | collective-permute-start | bytes 491528 | tf_op jit(solution)/shard_map/ppermute | solution.py:320
  77.8 0.0 collective-permute-done.5.refs_5_
  77.8 1.9 %collective-permute-start.6 = (bf16[16,40,128]{2,1,0:T(8,128)(2,1)S(1)}, bf16[16,40,128]{2,1,0:T(8,128)(2,1)S(1)}, u32[]{:S(2)}, u32[]{:S(2)}) collective-permute-start(bf16[16,40,128]{2,1,0:T(8,128)(2,1)S(1)} %collective-permute-done.5.refs_5_), channel_id=1, source_target_pairs={{0,8},{8,16},{16,24},{24,32},{32,40},{40,48},{48,56},{56,0},{1,9},... | collective-permute-start | bytes 491528 | tf_op jit(solution)/shard_map/ppermute | solution.py:317
  79.7 5.7 %all-to-all-done.2.rows_ref = bf16[16,16,128]{2,1,0:T(8,128)(2,1)S(1)} async-done(((bf16[16,16,128]{2,1,0:T(8,128)(2,1)}), bf16[16,16,128]{2,1,0:T(8,128)(2,1)S(1)}, u32[]{:S(2)}, u32[]{:S(2)}) %all-to-all-start.2) | async-done | bytes 65568 | tf_op jit(solution)/shard_map/all_to_all | solution.py:24
  85.4 0.7 shard_map.198
  86.2 9.1 %all-to-all-start.3 = ((f32[8,8,128]{2,1,0:T(8,128)}), f32[8,8,128]{2,1,0:T(8,128)S(1)}, u32[]{:S(2)}, u32[]{:S(2)}) async-start(f32[8,8,128]{2,1,0:T(8,128)} %shard_map.198), calls=%async_computation.3 | async-start | bytes 65536 | tf_op jit(solution)/shard_map/all_to_all | solution.py:24
  95.3 4.7 %all-to-all-done.3.squares_ref = f32[8,8,128]{2,1,0:T(8,128)S(1)} async-done(((f32[8,8,128]{2,1,0:T(8,128)}), f32[8,8,128]{2,1,0:T(8,128)S(1)}, u32[]{:S(2)}, u32[]{:S(2)}) %all-to-all-start.3) | async-done | bytes 32800 | tf_op jit(solution)/shard_map/all_to_all | solution.py:24
  100.0 0.0 collective-permute-done.2.refs_3_
  100.0 0.0 collective-permute-done.6.refs_4_
  100.1 0.0 copy-done.1
  100.1 2.3 %shard_map.199 = (f32[128,128]{1,0:T(8,128)}, f32[128,128]{1,0:T(8,128)}, f32[128,128]{1,0:T(8,128)}, f32[128,128]{1,0:T(8,128)}, bf16[2048,128]{1,0:T(8,128)(2,...) custom-call(s32[1]{0:T(128)} %bitcast.fs_ref, ...), custom_call_target="tpu_custom_call" | custom-call | flops 268435456 | bytes 1048576 | tf_op jit(solution)/shard_map/pallas_call | solution.py:153
  (4 shorter events, 0.0 us)
Async XLA Ops:
  0.6 4.9 %copy-start = (bf16[896,128]{1,0:T(8,128)(2,1)S(1)}, bf16[896,128]{1,0:T(8,128)(2,1)}, u32[]{:S(2)}) copy-start(bf16[896,128]{1,0:T(8,128)(2,1)} %param.13) | copy-start | bytes 688132
  0.7 3.5 %copy-start.2 = (bf16[2048,128]{1,0:T(8,128)(2,1)S(1)}, bf16[2048,128]{1,0:T(8,128)(2,1)}, u32[]{:S(2)}) copy-start(bf16[2048,128]{1,0:T(8,128)(2,1)} %basis_output_ref.1) | copy-start | bytes 1572868
  0.7 3.5 %copy-start.9 = (bf16[896,2048]{1,0:T(8,128)(2,1)S(1)}, bf16[896,2048]{1,0:T(8,128)(2,1)}, u32[]{:S(2)}) copy-start(bf16[896,2048]{1,0:T(8,128)(2,1)} %param.15) | copy-start | bytes 11010052
  4.2 1.6 %copy-start.10 = (bf16[896,128]{1,0:T(8,128)(2,1)S(1)}, bf16[896,128]{1,0:T(8,128)(2,1)}, u32[]{:S(2)}) copy-start(bf16[896,128]{1,0:T(8,128)(2,1)} %param.14) | copy-start | bytes 688132
  4.2 1.9 %copy-start.3 = (f32[128,128]{1,0:T(8,128)S(1)}, f32[128,128]{1,0:T(8,128)}, u32[]{:S(2)}) copy-start(f32[128,128]{1,0:T(8,128)} %weight_value_ref.3) | copy-start | bytes 196612
  4.2 1.9 %copy-start.4 = (f32[128,128]{1,0:T(8,128)S(1)}, f32[128,128]{1,0:T(8,128)}, u32[]{:S(2)}) copy-start(f32[128,128]{1,0:T(8,128)} %weight_output_ref.3) | copy-start | bytes 196612
  4.3 1.9 %copy-start.5 = (f32[8,128]{1,0:T(8,128)S(1)}, f32[8,128]{1,0:T(8,128)}, u32[]{:S(2)}) copy-start(f32[8,128]{1,0:T(8,128)} %first_value_ref.3) | copy-start | bytes 12292
  4.3 1.9 %copy-start.6 = (f32[8,128]{1,0:T(8,128)S(1)}, f32[8,128]{1,0:T(8,128)}, u32[]{:S(2)}) copy-start(f32[8,128]{1,0:T(8,128)} %second_value_ref.3) | copy-start | bytes 12292
  4.3 1.9 %copy-start.7 = (f32[8,128]{1,0:T(8,128)S(1)}, f32[8,128]{1,0:T(8,128)}, u32[]{:S(2)}) copy-start(f32[8,128]{1,0:T(8,128)} %first_output_ref.3) | copy-start | bytes 12292
  4.3 1.9 %copy-start.8 = (f32[8,128]{1,0:T(8,128)S(1)}, f32[8,128]{1,0:T(8,128)}, u32[]{:S(2)}) copy-start(f32[8,128]{1,0:T(8,128)} %second_output_ref.3) | copy-start | bytes 12292
  4.3 95.8 %copy-start.1 = (bf16[2048,128]{1,0:T(8,128)(2,1)S(1)}, bf16[2048,128]{1,0:T(8,128)(2,1)}, u32[]{:S(2)}) copy-start(bf16[2048,128]{1,0:T(8,128)(2,1)} %basis_value_ref.1) | copy-start | bytes 1572868
  38.7 7.8 %collective-permute-start.3 = (bf16[16,40,128]{2,1,0:T(8,128)(2,1)S(1)}, bf16[16,40,128]{2,1,0:T(8,128)(2,1)S(1)}, u32[]{:S(2)}, u32[]{:S(2)}) collective-permute-start(bf16[16,40,128]{2,1,0:T(8,128)(2,1)S(1)} %get-tuple-element.17.refs_0_), channel_id=1, source_target_pairs={{0,8},{8,16},{16,24},{24,32},{32,40},{40,48},{48,56},{56,0},{1,9},... | collective-permute-start | bytes 491528 | tf_op jit(solution)/shard_map/ppermute | solution.py:317
  41.9 13.1 %collective-permute-start = (bf16[16,40,128]{2,1,0:T(8,128)(2,1)S(1)}, bf16[16,40,128]{2,1,0:T(8,128)(2,1)S(1)}, u32[]{:S(2)}, u32[]{:S(2)}) collective-permute-start(bf16[16,40,128]{2,1,0:T(8,128)(2,1)S(1)} %get-tuple-element.17.refs_0_), channel_id=1, source_target_pairs={{0,56},{8,0},{16,8},{24,16},{32,24},{40,32},{48,40},{56,48},{1,57}... | collective-permute-start | bytes 491528 | tf_op jit(solution)/shard_map/ppermute | solution.py:320
  46.5 13.1 %collective-permute-start.4 = (bf16[16,40,128]{2,1,0:T(8,128)(2,1)S(1)}, bf16[16,40,128]{2,1,0:T(8,128)(2,1)S(1)}, u32[]{:S(2)}, u32[]{:S(2)}) collective-permute-start(bf16[16,40,128]{2,1,0:T(8,128)(2,1)S(1)} %collective-permute-done.3.refs_7_), channel_id=1, source_target_pairs={{0,8},{8,16},{16,24},{24,32},{32,40},{40,48},{48,56},{56,0},{1,9},... | collective-permute-start | bytes 491528 | tf_op jit(solution)/shard_map/ppermute | solution.py:317
  48.4 14.1 %all-to-all-start.1 = ((f32[8,16,128]{2,1,0:T(8,128)}), f32[8,16,128]{2,1,0:T(8,128)S(1)}, u32[]{:S(2)}, u32[]{:S(2)}) async-start(f32[8,16,128]{2,1,0:T(8,128)} %get-tuple-element.14), calls=%async_computation.1 | async-start | bytes 131072 | tf_op jit(solution)/shard_map/all_to_all | solution.py:24
  55.0 18.8 %collective-permute-start.1 = (bf16[16,40,128]{2,1,0:T(8,128)(2,1)S(1)}, bf16[16,40,128]{2,1,0:T(8,128)(2,1)S(1)}, u32[]{:S(2)}, u32[]{:S(2)}) collective-permute-start(bf16[16,40,128]{2,1,0:T(8,128)(2,1)S(1)} %collective-permute-done.refs_1_), channel_id=1, source_target_pairs={{0,56},{8,0},{16,8},{24,16},{32,24},{40,32},{48,40},{56,48},{1,57}... | collective-permute-start | bytes 491528 | tf_op jit(solution)/shard_map/ppermute | solution.py:320
  59.6 18.1 %collective-permute-start.5 = (bf16[16,40,128]{2,1,0:T(8,128)(2,1)S(1)}, bf16[16,40,128]{2,1,0:T(8,128)(2,1)S(1)}, u32[]{:S(2)}, u32[]{:S(2)}) collective-permute-start(bf16[16,40,128]{2,1,0:T(8,128)(2,1)S(1)} %collective-permute-done.4.refs_6_), channel_id=1, source_target_pairs={{0,8},{8,16},{16,24},{24,32},{32,40},{40,48},{48,56},{56,0},{1,9},... | collective-permute-start | bytes 491528 | tf_op jit(solution)/shard_map/ppermute | solution.py:317
  63.2 22.2 %all-to-all-start.2 = ((bf16[16,16,128]{2,1,0:T(8,128)(2,1)}), bf16[16,16,128]{2,1,0:T(8,128)(2,1)S(1)}, u32[]{:S(2)}, u32[]{:S(2)}) async-start(bf16[16,16,128]{2,1,0:T(8,128)(2,1)} %get-tuple-element.15), calls=%async_computation.2 | async-start | bytes 131072 | tf_op jit(solution)/shard_map/all_to_all | solution.py:24
  73.9 26.2 %collective-permute-start.2 = (bf16[16,40,128]{2,1,0:T(8,128)(2,1)S(1)}, bf16[16,40,128]{2,1,0:T(8,128)(2,1)S(1)}, u32[]{:S(2)}, u32[]{:S(2)}) collective-permute-start(bf16[16,40,128]{2,1,0:T(8,128)(2,1)S(1)} %collective-permute-done.1.refs_2_), channel_id=1, source_target_pairs={{0,56},{8,0},{16,8},{24,16},{32,24},{40,32},{48,40},{56,48},{1,57}... | collective-permute-start | bytes 491528 | tf_op jit(solution)/shard_map/ppermute | solution.py:320
  77.8 22.3 %collective-permute-start.6 = (bf16[16,40,128]{2,1,0:T(8,128)(2,1)S(1)}, bf16[16,40,128]{2,1,0:T(8,128)(2,1)S(1)}, u32[]{:S(2)}, u32[]{:S(2)}) collective-permute-start(bf16[16,40,128]{2,1,0:T(8,128)(2,1)S(1)} %collective-permute-done.5.refs_5_), channel_id=1, source_target_pairs={{0,8},{8,16},{16,24},{24,32},{32,40},{40,48},{48,56},{56,0},{1,9},... | collective-permute-start | bytes 491528 | tf_op jit(solution)/shard_map/ppermute | solution.py:317
  86.2 13.9 %all-to-all-start.3 = ((f32[8,8,128]{2,1,0:T(8,128)}), f32[8,8,128]{2,1,0:T(8,128)S(1)}, u32[]{:S(2)}, u32[]{:S(2)}) async-start(f32[8,8,128]{2,1,0:T(8,128)} %shard_map.198), calls=%async_computation.3 | async-start | bytes 65536 | tf_op jit(solution)/shard_map/all_to_all | solution.py:24
where the time goes:
time: 103 us; the launch traced here: 102 us
  starting transfers between devices  47.6 us (46%)
  blocking collectives  31.9 us (31%)
  waiting for transfers between devices  12.3 us (12%)
  matrix products  5.29 us (5%)
  Pallas kernels  4.42 us (4%)
    all_to_all x1, blocking collectives, exchange(): return lax.all_to_all(chunks, axes, 0, 0, tiled=True)  31.9 us
    all_to_all x3, starting transfers between devices, exchange(): return lax.all_to_all(chunks, axes, 0, 0, tiled=True)  26.4 us
    ppermute x3, starting transfers between devices, local(): down = lax.ppermute(down, 'rep', [(r, (r - 1) % rep) for r in range(rep)])  12.3 us
    all_to_all x3, waiting for transfers between devices, exchange(): return lax.all_to_all(chunks, axes, 0, 0, tiled=True)  11.5 us
    ppermute x4, starting transfers between devices, local(): up = lax.ppermute(up, 'rep', [(r, (r + 1) % rep) for r in range(rep)])  8.94 us
    pallas_call x5, Pallas kernels, call(): pl.pallas_call(kernel, out_shape=outs, in_specs=[vmem] * len(inputs) if s...  4.42 us
    dot_general x1, matrix products, partial(): reduced_hidden = jnp.dot(hidden, bases[0], preferred_element_type=f32)  3.51 us
  transfers between devices with their start and end apart: 10, of which 4 were waited for; matrix products, arithmetic and copies ran while one was open for 0% of the time, Pallas kernels for 1%

commit v1 on v0

--- a/solution.py
+++ b/solution.py
@@ -40,7 +40,6 @@
     fs_ref,
     rep_ref,
     rows_ref,
-    squares_ref,
     whole_ref,
     first_value_ref,
     second_value_ref,
@@ -70,7 +69,7 @@
         value_ref,
         output_ref,
     ) = refs
-    fs, _, columns = rows_ref.shape
+    fs, height, columns = rows_ref.shape
     ranks = first_value_ref.shape[0]
     count = 2 * ranks
     block = weight_value_ref.shape[0]
@@ -83,9 +82,11 @@
         old = piece_refs[away][:, 2 * cut :, :].astype(f32)
         olds_ref[other] = old[:, :part] + old[:, part:]
 
-    total = squares_ref[0]
-    for t in range(1, squares_ref.shape[0]):
-        total = total + squares_ref[t]
+    half = (height - count) // 2
+    total = rows_ref[0, count:, :].astype(f32)
+    for i in range(1, fs):
+        total = total + rows_ref[i, count:, :].astype(f32)
+    total = total[:half] + total[half:]
     mean_square = jnp.max(total, keepdims=True) / (2 * RANK * AW)
     clip_factor = jnp.minimum(1.0, 1.0 / jnp.sqrt(mean_square + norm_epsilon))
 
@@ -239,23 +240,27 @@
     pieces_ref[...] = mixed_ref[:, count:, :]
 
 
-def rows_kernel(sums_ref, whole_ref, out_ref):
+def squares_kernel(sums_ref, whole_ref, squares_ref):
     total = sums_ref[0]
     for j in range(1, sums_ref.shape[0]):
         total = total + sums_ref[j]
     whole_ref[...] = total
-    total = total.astype(bf16)
+    squares = jnp.sum(total * total, keepdims=True)
+    squares_ref[...] = jnp.broadcast_to(squares[None], squares_ref.shape)
+
+
+def rows_kernel(whole_ref, squares_ref, out_ref):
+    count = whole_ref.shape[0]
+    total = squares_ref[0]
+    for t in range(1, squares_ref.shape[0]):
+        total = total + squares_ref[t]
+    total = total[:4]
+    upper = total.astype(bf16).astype(f32)
+    total = jnp.concatenate([upper, total - upper]).astype(bf16)
+    whole = whole_ref[...].astype(bf16)
     for i in range(out_ref.shape[0]):
-        out_ref[i] = total
-
-
-def squares_kernel(rows_ref, out_ref):
-    total = jnp.zeros(rows_ref.shape[1:], f32)
-    for i in range(rows_ref.shape[0]):
-        row = rows_ref[i].astype(f32)
-        total = total + row * row
-    total = jnp.sum(total, keepdims=True)
-    out_ref[...] = jnp.broadcast_to(total[None], out_ref.shape)
+        out_ref[i, :count, :] = whole
+        out_ref[i, count:, :] = total
 
 
 def local(
@@ -303,13 +308,12 @@
         [((rep, count, columns), f32), ((fs, height, columns), bf16)],
     )
     summed = exchange(summed, "rep")
-    whole, rowed = call(
-        rows_kernel, (summed,), [((count, columns), f32), ((fs, count, columns), bf16)]
-    )
-
+    whole, squares = call(
+        squares_kernel, (summed,), [((count, columns), f32), ((tp, 8, columns), f32)]
+    )
+    squares = exchange(squares, "tp")
+    rowed = call(rows_kernel, (whole, squares), [((fs, count + 8, columns), bf16)])[0]
     gathered = exchange(rowed, "fs")
-    squares = call(squares_kernel, (gathered,), [((tp, 8, columns), f32)])[0]
-    squares = exchange(squares, "tp")
 
     pieces = [piece] + [None] * (rep - 1)
     up = down = piece
@@ -325,9 +329,9 @@
     shapes += [((depth, columns), bf16), ((rows, depth), bf16)] + [((ranks, columns), f32)] * 4
     return call(
         finish_kernel,
-        (fs_index, rep_index, gathered, squares, whole, *olds, *bases, *weights, *pieces),
+        (fs_index, rep_index, gathered, whole, *olds, *bases, *weights, *pieces),
         shapes,
-        specs=[smem] * 2 + [vmem] * (11 + rep),
+        specs=[smem] * 2 + [vmem] * (10 + rep),
         scratch=[
             pltpu.VMEM((rep, fs, 2 * (rows // rep), columns), bf16),
             pltpu.VMEM((rep, fs, 4 * ranks // rep, columns), f32),

time: 103 us -> 99.9 us (0.970)
  the two profiles are of different devices: /device:TPU:1 before, /device:TPU:6 now
where the time goes in v1:
time: 99.9 us; the launch traced here: 98.4 us
  blocking collectives  43.8 us (44%)
  starting transfers between devices  34.8 us (35%)
  waiting for transfers between devices  9.77 us (10%)
  matrix products  5.29 us (5%)
  Pallas kernels  3.8 us (4%)
    all_to_all x2, blocking collectives, exchange(): return lax.all_to_all(chunks, axes, 0, 0, tiled=True)  43.8 us
    ppermute x3, starting transfers between devices, local(): down = lax.ppermute(down, 'rep', [(r, (r - 1) % rep) for r in range(rep)])  13.8 us
    all_to_all x2, starting transfers between devices, exchange(): return lax.all_to_all(chunks, axes, 0, 0, tiled=True)  11.6 us
    ppermute x4, starting transfers between devices, local(): up = lax.ppermute(up, 'rep', [(r, (r + 1) % rep) for r in range(rep)])  9.41 us
    ppermute x4, waiting for transfers between devices, local(): up = lax.ppermute(up, 'rep', [(r, (r + 1) % rep) for r in range(rep)])  5.62 us
    pallas_call x5, Pallas kernels, call(): pl.pallas_call(kernel, out_shape=outs, in_specs=[vmem] * len(inputs) if s...  3.8 us
    dot_general x1, matrix products, partial(): reduced_hidden = jnp.dot(hidden, bases[0], preferred_element_type=f32)  3.51 us
    ppermute x3, waiting for transfers between devices, local(): down = lax.ppermute(down, 'rep', [(r, (r - 1) % rep) for r in range(rep)])  2.5 us
  transfers between devices with their start and end apart: 9, of which 4 were waited for; matrix products, arithmetic and copies ran while one was open for 0% of the time, Pallas kernels for 1%

profile of v1, /device:TPU:6, one launch (start us, length us, event | category | flops | bytes accessed | tf_op | source)
XLA Modules:
  0.0 98.4 jit_solution(14452919286350737017)
XLA Ops:
  0.6 0.0 copy-start
  0.7 0.0 copy-start.2
  0.7 0.0 copy-start.9
  0.7 3.5 %subtract_convert_fusion.1 = (bf16[896,128]{0,1:T(8,128)(2,1)S(1)}, bf16[896,128]{0,1:T(8,128)(2,1)S(1)}) fusion(bf16[896,2048]{1,0:T(8,128)(2,1)} %param.12, bf16[2048,128]{1,0:T(8,128)(2,1)} %basis_value_ref.1), kind=kOutput, calls=%fused_computation.9 | convolution fusion | flops 470220800 | bytes 4653056 | tf_op jit(solution)/shard_map/dot_general | solution.py:219
  4.2 0.0 copy-done.2
  4.2 0.0 copy-done.9
  4.2 0.0 copy-start.10
  4.2 0.0 copy-start.3
  4.2 0.0 copy-start.4
  4.3 0.0 copy-start.5
  4.3 0.0 copy-start.6
  4.3 0.0 copy-start.7
  4.3 0.0 copy-start.8
  4.3 0.0 copy-start.1
  4.3 1.2 %subtract_convert_fusion = (bf16[896,128]{0,1:T(8,128)(2,1)S(1)}, bf16[896,128]{0,1:T(8,128)(2,1)S(1)}) fusion(bf16[896,2048]{1,0:T(8,128)(2,1)S(1)} %copy-done.9, bf16[2048,128]{1,0:T(8,128)(2,1)S(1)} %copy-done.2), kind=kOutput, calls=%fused_computation.8 | convolution fusion | flops 470220800 | bytes 4653056 | tf_op jit(solution)/shard_map/dot_general | solution.py:220
  5.6 0.0 copy-done
  5.6 0.3 fusion.value_ref
  5.9 0.3 fusion.4.output_ref
  6.1 0.0 copy-done.3
  6.2 0.0 copy-done.4
  6.2 0.0 copy-done.5
  6.2 0.0 copy-done.6
  6.2 0.0 copy-done.7
  6.2 0.0 copy-done.8
  6.2 35.8 %all_to_all.20.mixed_ref = bf16[16,56,128]{2,1,0:T(8,128)(2,1)S(1)} all-to-all(bf16[16,56,128]{2,1,0:T(8,128)(2,1)S(1)} %shard_map.195), channel_id=1, replica_groups=mesh['fs'=16,'rep'=8,'tp'=8] {'fs'}, dimensions={0} | all-to-all | bytes 458752 | tf_op jit(solution)/shard_map/all_to_all | solution.py:24
  42.1 0.7 shard_map.196
  42.7 3.5 %collective-permute-start.3 = (bf16[16,40,128]{2,1,0:T(8,128)(2,1)S(1)}, bf16[16,40,128]{2,1,0:T(8,128)(2,1)S(1)}, u32[]{:S(2)}, u32[]{:S(2)}) collective-permute-start(bf16[16,40,128]{2,1,0:T(8,128)(2,1)S(1)} %get-tuple-element.17.refs_0_), channel_id=1, source_target_pairs={{0,8},{8,16},{16,24},{24,32},{32,40},{40,48},{48,56},{56,0},{1,9},... | collective-permute-start | bytes 491528 | tf_op jit(solution)/shard_map/ppermute | solution.py:321
  46.2 6.2 %all-to-all-start.1 = ((f32[8,16,128]{2,1,0:T(8,128)}), f32[8,16,128]{2,1,0:T(8,128)S(1)}, u32[]{:S(2)}, u32[]{:S(2)}) async-start(f32[8,16,128]{2,1,0:T(8,128)} %get-tuple-element.14), calls=%async_computation.1 | async-start | bytes 131072 | tf_op jit(solution)/shard_map/all_to_all | solution.py:24
  52.4 5.1 %collective-permute-start = (bf16[16,40,128]{2,1,0:T(8,128)(2,1)S(1)}, bf16[16,40,128]{2,1,0:T(8,128)(2,1)S(1)}, u32[]{:S(2)}, u32[]{:S(2)}) collective-permute-start(bf16[16,40,128]{2,1,0:T(8,128)(2,1)S(1)} %get-tuple-element.17.refs_0_), channel_id=1, source_target_pairs={{0,56},{8,0},{16,8},{24,16},{32,24},{40,32},{48,40},{56,48},{1,57}... | collective-permute-start | bytes 491528 | tf_op jit(solution)/shard_map/ppermute | solution.py:324
  57.5 0.0 collective-permute-done.3.refs_7_
  57.6 1.9 %collective-permute-start.4 = (bf16[16,40,128]{2,1,0:T(8,128)(2,1)S(1)}, bf16[16,40,128]{2,1,0:T(8,128)(2,1)S(1)}, u32[]{:S(2)}, u32[]{:S(2)}) collective-permute-start(bf16[16,40,128]{2,1,0:T(8,128)(2,1)S(1)} %collective-permute-done.3.refs_7_), channel_id=1, source_target_pairs={{0,8},{8,16},{16,24},{24,32},{32,40},{40,48},{48,56},{56,0},{1,9},... | collective-permute-start | bytes 491528 | tf_op jit(solution)/shard_map/ppermute | solution.py:321
  59.5 1.6 %all-to-all-done.1.sums_ref = f32[8,16,128]{2,1,0:T(8,128)S(1)} async-done(((f32[8,16,128]{2,1,0:T(8,128)}), f32[8,16,128]{2,1,0:T(8,128)S(1)}, u32[]{:S(2)}, u32[]{:S(2)}) %all-to-all-start.1) | async-done | bytes 65568 | tf_op jit(solution)/shard_map/all_to_all | solution.py:24
  61.1 0.1 shard_map.197
  61.3 7.9 %all_to_all.21.squares_ref = f32[8,8,128]{2,1,0:T(8,128)S(1)} all-to-all(f32[8,8,128]{2,1,0:T(8,128)S(1)} %get-tuple-element.16), channel_id=1, replica_groups=mesh['fs'=16,'rep'=8,'tp'=8] {'tp'}, dimensions={0} | all-to-all | bytes 65536 | tf_op jit(solution)/shard_map/all_to_all | solution.py:24
  69.2 0.7 shard_map.198
  69.9 5.3 %all-to-all-start.3 = ((bf16[16,24,128]{2,1,0:T(8,128)(2,1)}), bf16[16,24,128]{2,1,0:T(8,128)(2,1)S(1)}, u32[]{:S(2)}, u32[]{:S(2)}) async-start(bf16[16,24,128]{2,1,0:T(8,128)(2,1)} %shard_map.198), calls=%async_computation.3 | async-start | bytes 196608 | tf_op jit(solution)/shard_map/all_to_all | solution.py:24
  75.2 0.0 collective-permute-done.refs_1_
  75.2 3.7 %collective-permute-start.1 = (bf16[16,40,128]{2,1,0:T(8,128)(2,1)S(1)}, bf16[16,40,128]{2,1,0:T(8,128)(2,1)S(1)}, u32[]{:S(2)}, u32[]{:S(2)}) collective-permute-start(bf16[16,40,128]{2,1,0:T(8,128)(2,1)S(1)} %collective-permute-done.refs_1_), channel_id=1, source_target_pairs={{0,56},{8,0},{16,8},{24,16},{32,24},{40,32},{48,40},{56,48},{1,57}... | collective-permute-start | bytes 491528 | tf_op jit(solution)/shard_map/ppermute | solution.py:324
  79.0 0.0 collective-permute-done.4.refs_6_
  79.0 2.1 %collective-permute-start.5 = (bf16[16,40,128]{2,1,0:T(8,128)(2,1)S(1)}, bf16[16,40,128]{2,1,0:T(8,128)(2,1)S(1)}, u32[]{:S(2)}, u32[]{:S(2)}) collective-permute-start(bf16[16,40,128]{2,1,0:T(8,128)(2,1)S(1)} %collective-permute-done.4.refs_6_), channel_id=1, source_target_pairs={{0,8},{8,16},{16,24},{24,32},{32,40},{40,48},{48,56},{56,0},{1,9},... | collective-permute-start | bytes 491528 | tf_op jit(solution)/shard_map/ppermute | solution.py:321
  81.1 1.6 %collective-permute-done.1.refs_2_ = bf16[16,40,128]{2,1,0:T(8,128)(2,1)S(1)} collective-permute-done((bf16[16,40,128]{2,1,0:T(8,128)(2,1)S(1)}, bf16[16,40,128]{2,1,0:T(8,128)(2,1)S(1)}, u32[]{:S(2)}, u32[]{:S(2)}) %collective-permute-start.1) | collective-permute-done | bytes 163872 | tf_op jit(solution)/shard_map/ppermute | solution.py:324
  82.7 4.9 %collective-permute-start.2 = (bf16[16,40,128]{2,1,0:T(8,128)(2,1)S(1)}, bf16[16,40,128]{2,1,0:T(8,128)(2,1)S(1)}, u32[]{:S(2)}, u32[]{:S(2)}) collective-permute-start(bf16[16,40,128]{2,1,0:T(8,128)(2,1)S(1)} %collective-permute-done.1.refs_2_), channel_id=1, source_target_pairs={{0,56},{8,0},{16,8},{24,16},{32,24},{40,32},{48,40},{56,48},{1,57}... | collective-permute-start | bytes 491528 | tf_op jit(solution)/shard_map/ppermute | solution.py:324
  87.7 0.0 collective-permute-done.5.refs_5_
  87.7 1.9 %collective-permute-start.6 = (bf16[16,40,128]{2,1,0:T(8,128)(2,1)S(1)}, bf16[16,40,128]{2,1,0:T(8,128)(2,1)S(1)}, u32[]{:S(2)}, u32[]{:S(2)}) collective-permute-start(bf16[16,40,128]{2,1,0:T(8,128)(2,1)S(1)} %collective-permute-done.5.refs_5_), channel_id=1, source_target_pairs={{0,8},{8,16},{16,24},{24,32},{32,40},{40,48},{48,56},{56,0},{1,9},... | collective-permute-start | bytes 491528 | tf_op jit(solution)/shard_map/ppermute | solution.py:321
  89.6 0.9 collective-permute-done.2.refs_3_
  90.5 0.0 all-to-all-done.3.rows_ref
  90.5 5.6 %collective-permute-done.6.refs_4_ = bf16[16,40,128]{2,1,0:T(8,128)(2,1)S(1)} collective-permute-done((bf16[16,40,128]{2,1,0:T(8,128)(2,1)S(1)}, bf16[16,40,128]{2,1,0:T(8,128)(2,1)S(1)}, u32[]{:S(2)}, u32[]{:S(2)}) %collective-permute-start.6) | collective-permute-done | bytes 163872 | tf_op jit(solution)/shard_map/ppermute | solution.py:321
  96.1 2.3 %shard_map.199 = (f32[128,128]{1,0:T(8,128)}, f32[128,128]{1,0:T(8,128)}, f32[128,128]{1,0:T(8,128)}, f32[128,128]{1,0:T(8,128)}, bf16[2048,128]{1,0:T(8,128)(2,...) custom-call(s32[1]{0:T(128)} %bitcast.fs_ref, ...), custom_call_target="tpu_custom_call" | custom-call | flops 268435456 | bytes 1048576 | tf_op jit(solution)/shard_map/pallas_call | solution.py:154
  (3 shorter events, 0.0 us)
Async XLA Ops:
  0.6 4.9 %copy-start = (bf16[896,128]{1,0:T(8,128)(2,1)S(1)}, bf16[896,128]{1,0:T(8,128)(2,1)}, u32[]{:S(2)}) copy-start(bf16[896,128]{1,0:T(8,128)(2,1)} %param.13) | copy-start | bytes 688132
  0.7 3.5 %copy-start.2 = (bf16[2048,128]{1,0:T(8,128)(2,1)S(1)}, bf16[2048,128]{1,0:T(8,128)(2,1)}, u32[]{:S(2)}) copy-start(bf16[2048,128]{1,0:T(8,128)(2,1)} %basis_output_ref.1) | copy-start | bytes 1572868
  0.7 3.5 %copy-start.9 = (bf16[896,2048]{1,0:T(8,128)(2,1)S(1)}, bf16[896,2048]{1,0:T(8,128)(2,1)}, u32[]{:S(2)}) copy-start(bf16[896,2048]{1,0:T(8,128)(2,1)} %param.15) | copy-start | bytes 11010052
  4.2 1.6 %copy-start.10 = (bf16[896,128]{1,0:T(8,128)(2,1)S(1)}, bf16[896,128]{1,0:T(8,128)(2,1)}, u32[]{:S(2)}) copy-start(bf16[896,128]{1,0:T(8,128)(2,1)} %param.14) | copy-start | bytes 688132
  4.2 1.9 %copy-start.3 = (f32[128,128]{1,0:T(8,128)S(1)}, f32[128,128]{1,0:T(8,128)}, u32[]{:S(2)}) copy-start(f32[128,128]{1,0:T(8,128)} %weight_value_ref.3) | copy-start | bytes 196612
  4.2 1.9 %copy-start.4 = (f32[128,128]{1,0:T(8,128)S(1)}, f32[128,128]{1,0:T(8,128)}, u32[]{:S(2)}) copy-start(f32[128,128]{1,0:T(8,128)} %weight_output_ref.3) | copy-start | bytes 196612
  4.3 1.9 %copy-start.5 = (f32[8,128]{1,0:T(8,128)S(1)}, f32[8,128]{1,0:T(8,128)}, u32[]{:S(2)}) copy-start(f32[8,128]{1,0:T(8,128)} %first_value_ref.3) | copy-start | bytes 12292
  4.3 1.9 %copy-start.6 = (f32[8,128]{1,0:T(8,128)S(1)}, f32[8,128]{1,0:T(8,128)}, u32[]{:S(2)}) copy-start(f32[8,128]{1,0:T(8,128)} %second_value_ref.3) | copy-start | bytes 12292
  4.3 1.9 %copy-start.7 = (f32[8,128]{1,0:T(8,128)S(1)}, f32[8,128]{1,0:T(8,128)}, u32[]{:S(2)}) copy-start(f32[8,128]{1,0:T(8,128)} %first_output_ref.3) | copy-start | bytes 12292
  4.3 1.9 %copy-start.8 = (f32[8,128]{1,0:T(8,128)S(1)}, f32[8,128]{1,0:T(8,128)}, u32[]{:S(2)}) copy-start(f32[8,128]{1,0:T(8,128)} %second_output_ref.3) | copy-start | bytes 12292
  4.3 91.8 %copy-start.1 = (bf16[2048,128]{1,0:T(8,128)(2,1)S(1)}, bf16[2048,128]{1,0:T(8,128)(2,1)}, u32[]{:S(2)}) copy-start(bf16[2048,128]{1,0:T(8,128)(2,1)} %basis_value_ref.1) | copy-start | bytes 1572868
  42.7 14.8 %collective-permute-start.3 = (bf16[16,40,128]{2,1,0:T(8,128)(2,1)S(1)}, bf16[16,40,128]{2,1,0:T(8,128)(2,1)S(1)}, u32[]{:S(2)}, u32[]{:S(2)}) collective-permute-start(bf16[16,40,128]{2,1,0:T(8,128)(2,1)S(1)} %get-tuple-element.17.refs_0_), channel_id=1, source_target_pairs={{0,8},{8,16},{16,24},{24,32},{32,40},{40,48},{48,56},{56,0},{1,9},... | collective-permute-start | bytes 491528 | tf_op jit(solution)/shard_map/ppermute | solution.py:321
  46.2 14.9 %all-to-all-start.1 = ((f32[8,16,128]{2,1,0:T(8,128)}), f32[8,16,128]{2,1,0:T(8,128)S(1)}, u32[]{:S(2)}, u32[]{:S(2)}) async-start(f32[8,16,128]{2,1,0:T(8,128)} %get-tuple-element.14), calls=%async_computation.1 | async-start | bytes 131072 | tf_op jit(solution)/shard_map/all_to_all | solution.py:24
  52.4 22.8 %collective-permute-start = (bf16[16,40,128]{2,1,0:T(8,128)(2,1)S(1)}, bf16[16,40,128]{2,1,0:T(8,128)(2,1)S(1)}, u32[]{:S(2)}, u32[]{:S(2)}) collective-permute-start(bf16[16,40,128]{2,1,0:T(8,128)(2,1)S(1)} %get-tuple-element.17.refs_0_), channel_id=1, source_target_pairs={{0,56},{8,0},{16,8},{24,16},{32,24},{40,32},{48,40},{56,48},{1,57}... | collective-permute-start | bytes 491528 | tf_op jit(solution)/shard_map/ppermute | solution.py:324
  57.6 21.4 %collective-permute-start.4 = (bf16[16,40,128]{2,1,0:T(8,128)(2,1)S(1)}, bf16[16,40,128]{2,1,0:T(8,128)(2,1)S(1)}, u32[]{:S(2)}, u32[]{:S(2)}) collective-permute-start(bf16[16,40,128]{2,1,0:T(8,128)(2,1)S(1)} %collective-permute-done.3.refs_7_), channel_id=1, source_target_pairs={{0,8},{8,16},{16,24},{24,32},{32,40},{40,48},{48,56},{56,0},{1,9},... | collective-permute-start | bytes 491528 | tf_op jit(solution)/shard_map/ppermute | solution.py:321
  69.9 20.6 %all-to-all-start.3 = ((bf16[16,24,128]{2,1,0:T(8,128)(2,1)}), bf16[16,24,128]{2,1,0:T(8,128)(2,1)S(1)}, u32[]{:S(2)}, u32[]{:S(2)}) async-start(bf16[16,24,128]{2,1,0:T(8,128)(2,1)} %shard_map.198), calls=%async_computation.3 | async-start | bytes 196608 | tf_op jit(solution)/shard_map/all_to_all | solution.py:24
  75.2 7.5 %collective-permute-start.1 = (bf16[16,40,128]{2,1,0:T(8,128)(2,1)S(1)}, bf16[16,40,128]{2,1,0:T(8,128)(2,1)S(1)}, u32[]{:S(2)}, u32[]{:S(2)}) collective-permute-start(bf16[16,40,128]{2,1,0:T(8,128)(2,1)S(1)} %collective-permute-done.refs_1_), channel_id=1, source_target_pairs={{0,56},{8,0},{16,8},{24,16},{32,24},{40,32},{48,40},{56,48},{1,57}... | collective-permute-start | bytes 491528 | tf_op jit(solution)/shard_map/ppermute | solution.py:324
  79.0 8.7 %collective-permute-start.5 = (bf16[16,40,128]{2,1,0:T(8,128)(2,1)S(1)}, bf16[16,40,128]{2,1,0:T(8,128)(2,1)S(1)}, u32[]{:S(2)}, u32[]{:S(2)}) collective-permute-start(bf16[16,40,128]{2,1,0:T(8,128)(2,1)S(1)} %collective-permute-done.4.refs_6_), channel_id=1, source_target_pairs={{0,8},{8,16},{16,24},{24,32},{32,40},{40,48},{48,56},{56,0},{1,9},... | collective-permute-start | bytes 491528 | tf_op jit(solution)/shard_map/ppermute | solution.py:321
  82.7 7.8 %collective-permute-start.2 = (bf16[16,40,128]{2,1,0:T(8,128)(2,1)S(1)}, bf16[16,40,128]{2,1,0:T(8,128)(2,1)S(1)}, u32[]{:S(2)}, u32[]{:S(2)}) collective-permute-start(bf16[16,40,128]{2,1,0:T(8,128)(2,1)S(1)} %collective-permute-done.1.refs_2_), channel_id=1, source_target_pairs={{0,56},{8,0},{16,8},{24,16},{32,24},{40,32},{48,40},{56,48},{1,57}... | collective-permute-start | bytes 491528 | tf_op jit(solution)/shard_map/ppermute | solution.py:324
  87.7 8.4 %collective-permute-start.6 = (bf16[16,40,128]{2,1,0:T(8,128)(2,1)S(1)}, bf16[16,40,128]{2,1,0:T(8,128)(2,1)S(1)}, u32[]{:S(2)}, u32[]{:S(2)}) collective-permute-start(bf16[16,40,128]{2,1,0:T(8,128)(2,1)S(1)} %collective-permute-done.5.refs_5_), channel_id=1, source_target_pairs={{0,8},{8,16},{16,24},{24,32},{32,40},{40,48},{48,56},{56,0},{1,9},... | collective-permute-start | bytes 491528 | tf_op jit(solution)/shard_map/ppermute | solution.py:321
